TPU v7x, 512 devices: a whole 4x8x8 slice. The times are simulated.
512 devices in a mesh: ep: 32 (over z, x), tp: 16 (over y, core).
Axes of the slice: x: 4, y: 8, z: 8, core: 2. Of those that a mesh axis runs over, the one named last changes fastest.
Arguments:
- tokens: bfloat16 [8192, 2048], P('ep')
- norm_gain: float32 [2048], replicated, may hold values from 0.1 to 1.9
- chosen: int32 [32, 1024], replicated, may hold values from 0 to 8191, as said below
- route_weight: float32 [32, 1024], P('ep'), may hold values from 0.2 to 1
- gate_weight: bfloat16 [32, 2048, 4096], P('ep', None, 'tp'), may hold values from -0.125 to 0.125
- up_weight: bfloat16 [32, 2048, 4096], P('ep', None, 'tp'), may hold values from -0.125 to 0.125
- down_weight: bfloat16 [32, 4096, 2048], P('ep', 'tp'), may hold values from -0.09375 to 0.09375
Outputs:
- combined: bfloat16 [8192, 2048], P('ep', 'tp')
Inputs may be any that keep to these rules, and one draw needn't show every extreme that they name: Each row of chosen lists 1024 distinct token numbers in ascending order. Of the 256 consecutive tokens of one index of ep, a row holds at most 48, and every draw has rows that hold exactly 48 of them.
All inputs are finite; a program needn't handle non-finite values.
Results may differ from a plain program's by a relative error of at most 0.02.
Values may be sent and summed in bfloat16 or wider, within the bound.
No kernel may reach another device: no remote copies, remote signals or barrier semaphores. Data moves between devices by JAX's collectives and lax.ppermute only.
A program may use at most 64 MiB of HBM per device.

v0:
```python
import jax
import jax.numpy as jnp
from jax import lax
from jax.sharding import Mesh
from jax.sharding import PartitionSpec as P

EP = ("ep_0", "ep_1")


def whole_of(x, axes, dim):
    if not axes:
        return x
    nearer = lax.all_gather(x, axes[-1], axis=dim, tiled=True)
    return whole_of(nearer, axes[:-1], dim)


def shards(tokens, norm_gain, chosen, route_weight, gate_weight, up_weight, down_weight):
    tok_rows, row_width = tokens.shape
    experts, capacity = chosen.shape
    ep_count = lax.axis_size(EP)
    tp_count = lax.axis_size("tp")
    owner_index = lax.axis_index(EP)
    lane_index = lax.axis_index("tp")
    slot_most = 3 * tok_rows // 16
    col_width = row_width // tp_count
    values = tokens.astype(jnp.float32)
    scale = lax.rsqrt(jnp.mean(values * values, axis=-1, keepdims=True) + 1e-06)
    normed = (values * scale * norm_gain[None, :]).astype(jnp.bfloat16)
    slot_steps = jnp.arange(slot_most, dtype=jnp.int32)
    first_token = owner_index * tok_rows
    run_start = jnp.sum((chosen < first_token).astype(jnp.int32), axis=1)
    run_end = jnp.sum((chosen < first_token + tok_rows).astype(jnp.int32), axis=1)
    run_count = run_end - run_start
    slot_live = slot_steps[None, :] < run_count[:, None]
    slot_place = jnp.minimum(run_start[:, None] + slot_steps[None, :], capacity - 1)
    slot_token = jnp.take_along_axis(chosen, slot_place, axis=1) - first_token
    my_chosen = lax.dynamic_index_in_dim(chosen, owner_index, 0, keepdims=False)
    block_edges = jnp.arange(ep_count, dtype=jnp.int32) * tok_rows
    src_start = jnp.sum((my_chosen[None, :] < block_edges[:, None]).astype(jnp.int32), axis=1)
    src_end = jnp.concatenate([src_start[1:], jnp.full((1,), capacity, jnp.int32)])
    gate_mat = gate_weight[0]
    up_mat = up_weight[0]
    down_mat = down_weight[0]
    my_columns = lax.dynamic_slice_in_dim(normed, lane_index * col_width, col_width, 1)
    all_columns = whole_of(my_columns, EP, 0)
    picked_rows = all_columns[my_chosen]
    segment = lax.all_gather(picked_rows, "tp", axis=1, tiled=True)
    gate_pre = jnp.dot(segment, gate_mat, preferred_element_type=jnp.float32)
    up_pre = jnp.dot(segment, up_mat, preferred_element_type=jnp.float32)
    hidden = (jax.nn.silu(gate_pre) * up_pre).astype(jnp.bfloat16)
    summed_out = lax.psum_scatter(
        lax.dot_general(
            down_mat, hidden, (((0,), (1,)), ((), ())), preferred_element_type=jnp.float32
        ).astype(jnp.bfloat16),
        "tp",
        scatter_dimension=0,
        tiled=True,
    ).astype(jnp.float32)
    weighted = (summed_out.T * route_weight[0][:, None]).astype(jnp.bfloat16)
    back_place = jnp.minimum(src_start[:, None] + slot_steps[None, :], capacity - 1)
    back_live = slot_steps[None, :] < (src_end - src_start)[:, None]
    outgoing_back = jnp.where(
        back_live[:, :, None], weighted[back_place], jnp.zeros((), jnp.bfloat16)
    )
    returned = lax.all_to_all(outgoing_back, EP, split_axis=0, concat_axis=0, tiled=True)
    target_row = jnp.where(slot_live, slot_token, tok_rows).reshape(-1)
    placement = (jnp.arange(tok_rows, dtype=jnp.int32)[:, None] == target_row[None, :]).astype(
        jnp.bfloat16
    )
    combined = jnp.dot(
        placement, returned.reshape(-1, col_width), preferred_element_type=jnp.float32
    )
    return combined.astype(jnp.bfloat16)


def solution(mesh):
    finer = Mesh(mesh.devices.reshape(8, 4, mesh.shape["tp"]), ("ep_0", "ep_1", "tp"))
    in_specs = (
        P(EP, None),
        P(),
        P(),
        P(EP, None),
        P(EP, None, "tp"),
        P(EP, None, "tp"),
        P(EP, "tp", None),
    )
    out_specs = P(EP, "tp")
    return jax.shard_map(
        shards, mesh=finer, in_specs=in_specs, out_specs=out_specs, check_vma=False
    )
```

profile of v0, /device:TPU:2, one launch (start us, length us, event | category | flops | bytes accessed | tf_op | source)
XLA Modules:
  0.0 248.7 jit_solution(2484285183497416496)
XLA Ops:
  6.5 1.5 convert_element_type.40
  8.1 1.5 multiply_reduce_fusion
  9.6 0.8 dynamic-slice
  10.4 0.1 fusion.17
  10.5 15.7 %all_gather.9 = bf16[1024,128]{1,0:T(8,128)(2,1)} all-gather(bf16[256,128]{1,0:T(8,128)(2,1)S(1)} %fusion.17), channel_id=1, replica_groups=mesh['ep_0'=8,'ep_1'=4,'tp'=16] {'ep_1'}, dimensions={0}, use_global_device_ids=true | all-gather | bytes 327680 | tf_op jit(solution)/shard_map/all_gather | solution.py:13
  26.3 46.0 %all-gather.4.cloned.1.call-done = bf16[8192,128]{1,0:T(8,128)(2,1)} async-done(((bf16[1024,128]{1,0:T(8,128)(2,1)}), bf16[8192,128]{1,0:T(8,128)(2,1)}) %all-gather.4.cloned.1.call-update) | async-done | bytes 2097168 | tf_op jit(solution)/shard_map/all_gather | solution.py:13
  72.3 5.9 %gather_fusion = bf16[1024,128]{1,0:T(8,128)(2,1)} fusion(bf16[8192,128]{1,0:T(8,128)(2,1)} %all-gather.4.cloned.1.call-done, s32[1024]{0:T(1024)S(1)} %broadcast_clamp_fusion), kind=kCustom, calls=%fused_computation | custom fusion | bytes 528384 | tf_op jit(solution)/shard_map/gather | solution.py:46
  78.3 49.9 %all-gather.6.cloned.1.call-done = bf16[1024,2048]{1,0:T(8,128)(2,1)} async-done(((bf16[1024,128]{1,0:T(8,128)(2,1)}), bf16[1024,2048]{1,0:T(8,128)(2,1)}) %all-gather.6.cloned.1.call-update) | async-done | bytes 4194320 | tf_op jit(solution)/shard_map/all_gather | solution.py:47
  128.2 3.7 %fusion.6 = f32[1024,256]{1,0:T(8,128)S(1)} fusion(bf16[1024,2048]{1,0:T(8,128)(2,1)} %all-gather.6.cloned.1.call-done, bf16[1,2048,256]{2,1,0:T(8,128)(2,1)} %param.11), kind=kOutput, calls=%fused_computation.12 | convolution fusion | flops 1073741824 | bytes 6291456 | tf_op jit(solution)/shard_map/dot_general | solution.py:48
  132.0 8.5 %convert_bitcast_fusion = bf16[2048,1024]{0,1:T(8,128)(2,1)} fusion(bf16[1024,2048]{1,0:T(8,128)(2,1)} %all-gather.6.cloned.1.call-done, bf16[1,256,2048]{2,1,0:T(8,128)(2,1)S(1)} %copy-done, bf16[1,2048,256]{2,1,0:T(8,128)(2,1)S(1)} %copy-done.3, f32[1024,256]{1,0:T(8,128)S(1)} %fusion.6), kind=kOutput, calls=%fused_computation.3 | convolution fusion | flops 2151153664 | bytes 11534336 | tf_op jit(solution)/shard_map/dot_general | solution.py:52
  140.5 6.4 %copy.8 = bf16[2048,1024]{1,0:T(8,128)(2,1)} copy(bf16[2048,1024]{0,1:T(8,128)(2,1)} %convert_bitcast_fusion) | data formatting | bytes 8388608
  146.9 0.2 convert_reduce_fusion
  147.1 0.1 slice.3
  147.2 0.1 compare_select_fusion
  147.3 0.1 reshape.234
  147.4 0.1 add_subtract_fusion
  147.4 0.1 iota_compare_fusion.4
  147.5 64.2 %reduce-scatter.4.cloned.1.call-done = bf16[128,1024]{1,0:T(8,128)(2,1)} async-done(((bf16[2048,1024]{1,0:T(8,128)(2,1)}), bf16[128,1024]{1,0:T(8,128)(2,1)}) %reduce-scatter.4.cloned.1.call-update) | async-done | bytes 262160
  211.7 1.1 copy.9
  212.8 0.2 fusion.15
  213.0 3.2 %gather_fusion.1 = bf16[1536,128]{1,0:T(8,128)(2,1)S(1)} fusion(bf16[1024,128]{1,0:T(8,128)(2,1)S(1)} %fusion.15, s32[2048]{0:T(1024)S(1)} %pad_clamp_fusion), kind=kCustom, calls=%fused_computation.1 | custom fusion | bytes 792576 | tf_op jit(solution)/shard_map/gather | solution.py:63
  216.2 1.0 broadcast_select_fusion
  217.3 10.5 %all-to-all-start = ((bf16[32,48,128]{2,1,0:T(8,128)(2,1)}), bf16[32,48,128]{2,1,0:T(8,128)(2,1)S(1)}, u32[]{:S(2)}, u32[]{:S(2)}) async-start(bf16[32,48,128]{2,1,0:T(8,128)(2,1)} %broadcast_select_fusion), calls=%async_computation | async-start | bytes 786432 | tf_op jit(solution)/shard_map/all_to_all | solution.py:65
  227.8 0.1 convert_reduce_fusion.1
  227.9 0.1 iota_compare_fusion.5
  228.0 0.1 lt.135
  228.1 0.1 fusion.20
  228.2 0.1 reshape.240
  228.2 12.6 %gather_fusion.2 = s32[1536]{0:T(1024)S(1)} fusion(s32[32,1024]{1,0:T(8,128)S(1)} %copy-done.1, s32[1536]{0:T(1024)S(1)} %reshape.240), kind=kCustom, calls=%fused_computation.2 | custom fusion | bytes 24576 | tf_op jit(solution)/shard_map/jit(take_along_axis)/gather | solution.py:36
  240.9 0.1 add.130
  241.0 0.1 lt.137
  241.1 1.0 fusion.2
  (24 shorter events, 0.3 us)
Async XLA Ops:
  6.5 125.4 %copy-start = (bf16[1,256,2048]{2,1,0:T(8,128)(2,1)S(1)}, bf16[1,256,2048]{2,1,0:T(8,128)(2,1)}, u32[]{:S(2)}) copy-start(bf16[1,256,2048]{2,1,0:T(8,128)(2,1)} %param.13) | copy-start | bytes 3145732
  6.5 19.7 %copy-start.1 = (s32[32,1024]{1,0:T(8,128)S(1)}, s32[32,1024]{1,0:T(8,128)}, u32[]{:S(2)}) copy-start(s32[32,1024]{1,0:T(8,128)} %param.9) | copy-start | bytes 393220
  6.5 65.7 %all-gather.4.cloned.1.call-start = ((), (), s32[]{:S(2)}) async-start(), calls=%async_computation.2 | async-start | bytes 2359296 | tf_op jit(solution)/shard_map/all_gather | solution.py:13
  26.2 102.0 %all-gather.6.cloned.1.call-start = ((), (), s32[]{:S(2)}) async-start(), calls=%async_computation.3 | async-start | bytes 4456448 | tf_op jit(solution)/shard_map/all_gather | solution.py:47
  78.2 53.8 %copy-start.3 = (bf16[1,2048,256]{2,1,0:T(8,128)(2,1)S(1)}, bf16[1,2048,256]{2,1,0:T(8,128)(2,1)}, u32[]{:S(2)}) copy-start(bf16[1,2048,256]{2,1,0:T(8,128)(2,1)} %param.12) | copy-start | bytes 3145732
  78.2 133.5 %reduce-scatter.4.cloned.1.call-start = ((), (), s32[]{:S(2)}) async-start(), calls=%async_computation.4 | async-start | bytes 4456448
  146.9 65.9 %copy-start.2 = (f32[1,1024]{1,0:T(1,128)S(1)}, f32[1,1024]{1,0:T(1,128)}, u32[]{:S(2)}) copy-start(f32[1,1024]{1,0:T(1,128)} %param.10) | copy-start | bytes 12292
  217.3 23.9 %all-to-all-start = ((bf16[32,48,128]{2,1,0:T(8,128)(2,1)}), bf16[32,48,128]{2,1,0:T(8,128)(2,1)S(1)}, u32[]{:S(2)}, u32[]{:S(2)}) async-start(bf16[32,48,128]{2,1,0:T(8,128)(2,1)} %broadcast_select_fusion), calls=%async_computation | async-start | bytes 786432 | tf_op jit(solution)/shard_map/all_to_all | solution.py:65
Sparse Core Ops, SparseCore 0:
  26.3 45.9 all-gather.3
  78.3 49.8 all-gather.5
  147.0 64.5 reduce-scatter.3
where the time goes:
time: 249 us
  waiting for transfers between devices  160 us (64%)
  local copies, waits for them, and re-layouts  30.6 us (12%)
  blocking collectives  15.7 us (6%)
  matrix products  13.3 us (5%)
  between operations  13.3 us (5%)
  starting transfers between devices  10.6 us (4%)
  other arithmetic  5.16 us (2%)
    unnamed x4, waiting for transfers between devices  64.2 us
    all_gather x1, waiting for transfers between devices, shards(): segment = lax.all_gather(picked_rows, 'tp', axis=1, tiled=True)  49.9 us
    all_gather x1, waiting for transfers between devices, whole_of(): nearer = lax.all_gather(x, axes[-1], axis=dim, tiled=True)  46 us
    all_gather x1, blocking collectives, whole_of(): nearer = lax.all_gather(x, axes[-1], axis=dim, tiled=True)  15.7 us
    gather x2, local copies, waits for them, and re-layouts, shards(): slot_token = jnp.take_along_axis(chosen, slot_place, axis=1) - first_token  12.7 us
    all_to_all x1, starting transfers between devices, shards(): lax.all_to_all(outgoing_back, EP, split_axis=0, concat_axis=0, tiled=True)  10.5 us
    dot_general x1, matrix products, shards(): lax.dot_general(down_mat, hidden, (((0,), (1,)), ((), ())), preferred_ele...  8.52 us
    unnamed x10, local copies, waits for them, and re-layouts  7.53 us
  transfers between devices with their start and end apart: 4, of which 3 were waited for; matrix products, arithmetic and copies ran while one was open for 6% of the time, Pallas kernels for 0%

commit v1 on v0

--- a/solution.py
+++ b/solution.py
@@ -44,7 +44,9 @@
     my_columns = lax.dynamic_slice_in_dim(normed, lane_index * col_width, col_width, 1)
     all_columns = whole_of(my_columns, EP, 0)
     picked_rows = all_columns[my_chosen]
-    segment = lax.all_gather(picked_rows, "tp", axis=1, tiled=True)
+    segment = jnp.concatenate(
+        lax.all_to_all(jnp.stack([picked_rows] * lax.axis_size("tp")), "tp", 0, 0), axis=1
+    )
     gate_pre = jnp.dot(segment, gate_mat, preferred_element_type=jnp.float32)
     up_pre = jnp.dot(segment, up_mat, preferred_element_type=jnp.float32)
     hidden = (jax.nn.silu(gate_pre) * up_pre).astype(jnp.bfloat16)

time: 249 us -> 298 us (1.20)
  blocking collectives: 15.7 us -> 117 us
  waiting for transfers between devices: 160 us -> 107 us
    all_to_all x0 -> x1, blocking collectives: none -> 101 us  [shards(): lax.all_to_all(jnp.stack([picked_rows] * lax.axis_size('tp')), 'tp', 0, 0)]
    all_gather x1 -> x0, waiting for transfers between devices: 49.9 us -> none  [shards(): segment = lax.all_gather(picked_rows, 'tp', axis=1, tiled=True)]
    unnamed x4 -> x3, waiting for transfers between devices: 64.2 us -> 61 us
    unnamed x10 -> x14, local copies, waits for them, and re-layouts: 7.53 us -> 9.51 us
  transfers between devices with their start and end apart: 4 -> 3, of which waited for: 3 -> 2; matrix products, arithmetic and copies ran while one was open for 6% -> 5% of each run, Pallas kernels for 0% -> 0%
where the time goes in v1:
time: 298 us; the launch traced here: 297 us
  blocking collectives  117 us (39%)
  waiting for transfers between devices  107 us (36%)
  local copies, waits for them, and re-layouts  32 us (11%)
  between operations  13.6 us (5%)
  matrix products  12.1 us (4%)
  starting transfers between devices  10.6 us (4%)
  other arithmetic  5.15 us (2%)
    all_to_all x1, blocking collectives, shards(): lax.all_to_all(jnp.stack([picked_rows] * lax.axis_size('tp')), 'tp', 0, 0)  101 us
    unnamed x3, waiting for transfers between devices  61 us
    all_gather x1, waiting for transfers between devices, whole_of(): nearer = lax.all_gather(x, axes[-1], axis=dim, tiled=True)  46 us
    all_gather x1, blocking collectives, whole_of(): nearer = lax.all_gather(x, axes[-1], axis=dim, tiled=True)  15.7 us
    gather x2, local copies, waits for them, and re-layouts, shards(): slot_token = jnp.take_along_axis(chosen, slot_place, axis=1) - first_token  12.7 us
    all_to_all x1, starting transfers between devices, shards(): lax.all_to_all(outgoing_back, EP, split_axis=0, concat_axis=0, tiled=True)  10.5 us
    unnamed x14, local copies, waits for them, and re-layouts  9.51 us
    dot_general x1, matrix products, shards(): lax.dot_general(down_mat, hidden, (((0,), (1,)), ((), ())), preferred_ele...  8.8 us
  transfers between devices with their start and end apart: 3, of which 2 were waited for; matrix products, arithmetic and copies ran while one was open for 5% of the time, Pallas kernels for 0%

profile of v1, /device:TPU:2, one launch (start us, length us, event | category | flops | bytes accessed | tf_op | source)
XLA Modules:
  0.0 297.5 jit_solution(8169380558942679593)
XLA Ops:
  6.5 1.5 convert_element_type.40
  8.1 1.5 multiply_reduce_fusion
  9.6 0.8 dynamic-slice
  10.4 0.1 fusion.17
  10.5 15.7 %all_gather.6 = bf16[1024,128]{1,0:T(8,128)(2,1)} all-gather(bf16[256,128]{1,0:T(8,128)(2,1)S(1)} %fusion.17), channel_id=1, replica_groups=mesh['ep_0'=8,'ep_1'=4,'tp'=16] {'ep_1'}, dimensions={0}, use_global_device_ids=true | all-gather | bytes 327680 | tf_op jit(solution)/shard_map/all_gather | solution.py:13
  26.3 46.0 %all-gather.2.cloned.1.call-done = bf16[8192,128]{1,0:T(8,128)(2,1)} async-done(((bf16[1024,128]{1,0:T(8,128)(2,1)}), bf16[8192,128]{1,0:T(8,128)(2,1)}) %all-gather.2.cloned.1.call-update) | async-done | bytes 2097168 | tf_op jit(solution)/shard_map/all_gather | solution.py:13
  72.3 4.7 %gather_fusion = bf16[1024,128]{1,0:T(8,128)(2,1)S(1)} fusion(bf16[8192,128]{1,0:T(8,128)(2,1)} %all-gather.2.cloned.1.call-done, s32[1024]{0:T(1024)S(1)} %broadcast_clamp_fusion), kind=kCustom, calls=%fused_computation | custom fusion | bytes 528384 | tf_op jit(solution)/shard_map/gather | solution.py:46
  77.0 0.1 copy.10
  77.2 0.5 stack.2
  77.7 101.4 %all_to_all.10 = bf16[16,1024,128]{1,2,0:T(8,128)(2,1)S(1)} all-to-all(bf16[16,1024,128]{1,2,0:T(8,128)(2,1)S(1)} %stack.2), channel_id=1, replica_groups=mesh['ep_0'=8,'ep_1'=4,'tp'=16] {'tp'}, dimensions={0} | all-to-all | bytes 8388608 | tf_op jit(solution)/shard_map/all_to_all | solution.py:48
  179.1 2.0 copy-done.2
  181.0 2.3 fusion.6
  183.4 8.8 %convert_bitcast_fusion = bf16[2048,1024]{0,1:T(8,128)(2,1)} fusion(bf16[1024,2048]{0,1:T(8,128)(2,1)} %bitcast.37, bf16[1,256,2048]{2,1,0:T(8,128)(2,1)S(1)} %copy-done, bf16[1,2048,256]{2,1,0:T(8,128)(2,1)S(1)} %copy-done.5, f32[1024,256]{1,0:T(8,128)} %fusion.6), kind=kOutput, calls=%fused_computation.3 | convolution fusion | flops 2151153664 | bytes 11534336 | tf_op jit(solution)/shard_map/dot_general | solution.py:54
  192.2 6.4 %copy.11 = bf16[2048,1024]{1,0:T(8,128)(2,1)} copy(bf16[2048,1024]{0,1:T(8,128)(2,1)} %convert_bitcast_fusion) | data formatting | bytes 8388608
  198.6 0.2 convert_reduce_fusion
  198.8 0.1 slice.3
  198.9 0.1 compare_select_fusion
  199.0 0.1 reshape.244
  199.1 0.1 add_subtract_fusion
  199.1 0.1 iota_compare_fusion.4
  199.2 61.0 %reduce-scatter.4.cloned.1.call-done = bf16[128,1024]{1,0:T(8,128)(2,1)} async-done(((bf16[2048,1024]{1,0:T(8,128)(2,1)}), bf16[128,1024]{1,0:T(8,128)(2,1)}) %reduce-scatter.4.cloned.1.call-update) | async-done | bytes 262160
  260.2 1.1 copy.12
  261.3 0.2 fusion.15
  261.5 3.2 %gather_fusion.1 = bf16[1536,128]{1,0:T(8,128)(2,1)S(1)} fusion(bf16[1024,128]{1,0:T(8,128)(2,1)S(1)} %fusion.15, s32[2048]{0:T(1024)S(1)} %pad_clamp_fusion), kind=kCustom, calls=%fused_computation.1 | custom fusion | bytes 792576 | tf_op jit(solution)/shard_map/gather | solution.py:65
  264.7 1.0 broadcast_select_fusion
  265.7 10.5 %all-to-all-start.1 = ((bf16[32,48,128]{2,1,0:T(8,128)(2,1)}), bf16[32,48,128]{2,1,0:T(8,128)(2,1)S(1)}, u32[]{:S(2)}, u32[]{:S(2)}) async-start(bf16[32,48,128]{2,1,0:T(8,128)(2,1)} %broadcast_select_fusion), calls=%async_computation.1 | async-start | bytes 786432 | tf_op jit(solution)/shard_map/all_to_all | solution.py:67
  276.3 0.1 convert_reduce_fusion.1
  276.5 0.1 lt.135
  276.6 0.1 fusion.20
  276.7 12.6 %gather_fusion.2 = s32[1536]{0:T(1024)S(1)} fusion(s32[32,1024]{1,0:T(8,128)S(1)} %copy-done.1, s32[1536]{0:T(1024)S(1)} %reshape.250), kind=kCustom, calls=%fused_computation.2 | custom fusion | bytes 24576 | tf_op jit(solution)/shard_map/jit(take_along_axis)/gather | solution.py:36
  289.4 0.1 add.130
  289.6 1.0 fusion.2
  (28 shorter events, 0.5 us)
Async XLA Ops:
  6.5 176.8 %copy-start = (bf16[1,256,2048]{2,1,0:T(8,128)(2,1)S(1)}, bf16[1,256,2048]{2,1,0:T(8,128)(2,1)}, u32[]{:S(2)}) copy-start(bf16[1,256,2048]{2,1,0:T(8,128)(2,1)} %param.13) | copy-start | bytes 3145732
  6.5 19.7 %copy-start.1 = (s32[32,1024]{1,0:T(8,128)S(1)}, s32[32,1024]{1,0:T(8,128)}, u32[]{:S(2)}) copy-start(s32[32,1024]{1,0:T(8,128)} %param.9) | copy-start | bytes 393220
  6.5 65.7 %all-gather.2.cloned.1.call-start = ((), (), s32[]{:S(2)}) async-start(), calls=%async_computation.3 | async-start | bytes 2359296 | tf_op jit(solution)/shard_map/all_gather | solution.py:13
  26.2 234.0 %reduce-scatter.4.cloned.1.call-start = ((), (), s32[]{:S(2)}) async-start(), calls=%async_computation.4 | async-start | bytes 4456448
  77.7 103.3 %copy-start.4 = (bf16[1,2048,256]{2,1,0:T(8,128)(2,1)S(1)}, bf16[1,2048,256]{2,1,0:T(8,128)(2,1)}, u32[]{:S(2)}) copy-start(bf16[1,2048,256]{2,1,0:T(8,128)(2,1)} %param.11) | copy-start | bytes 3145732
  179.1 2.0 copy-start.2
  181.0 2.3 copy-start.5
  198.6 62.7 %copy-start.3 = (f32[1,1024]{1,0:T(1,128)S(1)}, f32[1,1024]{1,0:T(1,128)}, u32[]{:S(2)}) copy-start(f32[1,1024]{1,0:T(1,128)} %param.10) | copy-start | bytes 12292
  265.7 23.9 %all-to-all-start.1 = ((bf16[32,48,128]{2,1,0:T(8,128)(2,1)}), bf16[32,48,128]{2,1,0:T(8,128)(2,1)S(1)}, u32[]{:S(2)}, u32[]{:S(2)}) async-start(bf16[32,48,128]{2,1,0:T(8,128)(2,1)} %broadcast_select_fusion), calls=%async_computation.1 | async-start | bytes 786432 | tf_op jit(solution)/shard_map/all_to_all | solution.py:67
Sparse Core Ops, SparseCore 0:
  26.3 45.9 all-gather.1
  198.7 61.3 reduce-scatter.3
